TPU v7x, 32 devices: a whole 2x2x4 slice. The times are simulated.
32 devices in a mesh: sp: 8 (over z, y), tp: 4 (over x, core).
Axes of the slice: x: 2, y: 2, z: 4, core: 2. Of those that a mesh axis runs over, the one named last changes fastest.
Arguments:
- tokens: bfloat16 [256, 48, 1024], P('sp', 'tp'), may hold values from -6 to 6
- norm_gain: float32 [1024], replicated, may hold values from 0.1 to 1.9
- x_weight: bfloat16 [1024, 1024], P(('sp', 'tp')), may hold values from -0.1875 to 0.1875
- gate_weight: bfloat16 [1024, 1024], P(('sp', 'tp')), may hold values from -0.1875 to 0.1875
- conv_taps: float32 [4, 1024], replicated, may hold values from -3 to 3
- rate_map: bfloat16 [2, 1024, 128], P(None, ('sp', 'tp')), may hold values from -0.5 to 0.5
- input_map: bfloat16 [2, 1024, 128], P(None, ('sp', 'tp')), may hold values from -0.5 to 0.5
- decay_rate: float32 [2, 1024], replicated, may hold values from 0.1 to 3
- out_weight: bfloat16 [1024, 1024], P(None, ('sp', 'tp')), may hold values from -0.5 to 0.5
Outputs:
- mixed_out: bfloat16 [256, 48, 1024], P('sp', 'tp')
All inputs are finite; a program needn't handle non-finite values.
Results may differ from a plain program's by a relative error of at most 0.004.
Values may be sent and summed in bfloat16 or wider, within the bound.
A program may use at most 128 MiB of HBM per device.

v0:
```python
import jax
import jax.numpy as jnp
from jax import lax
from jax.sharding import PartitionSpec as P

epsilon = 1e-06


def taken_in(shard, axis, dim, absorb, state):
    everything = jax.tree.map(lambda a: lax.all_gather(a, axis, axis=dim, tiled=True), shard)
    return absorb(state, everything, jnp.int32(0))


def extended_2(cells, sides, width, closed):
    for axis, dim in sides:
        count = lax.axis_size(axis)
        ends = count if closed else count - 1
        head = lax.slice_in_dim(cells, 0, width, axis=dim)
        tail = lax.slice_in_dim(cells, cells.shape[dim] - width, cells.shape[dim], axis=dim)
        cells = jnp.concatenate(
            [
                lax.ppermute(tail, axis, [(i, (i + 1) % count) for i in range(ends)]),
                cells,
                lax.ppermute(head, axis, [((i + 1) % count, i) for i in range(ends)]),
            ],
            axis=dim,
        )
    return cells


def carried_in(value, axis, join, neutral, backward):
    count, mine = lax.axis_size(axis), lax.axis_index(axis)
    pieces = jax.tree.map(lambda part: lax.all_gather(part, axis), value)
    if backward:
        pieces = jax.tree.map(lambda part: part[::-1], pieces)
        mine = count - 1 - mine
    so_far = jax.tree.map(
        lambda part, zero: jnp.full_like(part, 0) + jnp.asarray(zero, part.dtype), value, neutral
    )

    def lap(position, so_far):
        longer = join(so_far, jax.tree.map(lambda part: part[position], pieces))
        return jax.tree.map(lambda new, old: jnp.where(position < mine, new, old), longer, so_far)

    return lax.fori_loop(0, count - 1, lap, so_far)


def on_whole(shard, axis, dim, work):
    return work(lax.all_gather(shard, axis, axis=dim, tiled=True), jnp.int32(0))


def compose(earlier, later):
    return (earlier[0] * later[0], later[0] * earlier[1] + later[1])


def drive_terms(conv_bf, conv_f, rate_block, input_block, speed, seq_total):
    steps_here, seqs, channels = conv_bf.shape
    nblk = rate_block.shape[0]
    grouped = conv_bf.reshape(steps_here, seqs, nblk, -1)
    rate_gate = jax.nn.sigmoid(
        jnp.einsum("tsnc,ncd->tsnd", grouped, rate_block, preferred_element_type=jnp.float32)
    ).reshape(steps_here, seqs, channels)
    input_gate = jax.nn.sigmoid(
        jnp.einsum("tsnc,ncd->tsnd", grouped, input_block, preferred_element_type=jnp.float32)
    ).reshape(steps_here, seqs, channels)
    log_decay = -2.0 * rate_gate * speed / seq_total
    decay = jnp.exp(log_decay)
    drive = jnp.sqrt(-jnp.expm1(2.0 * log_decay)) * input_gate * conv_f
    return (decay, drive, log_decay)


def summarize(drive, log_decay, reverse):
    running = lax.cumsum(log_decay, axis=0, reverse=reverse)
    total_log = running[0] if reverse else running[-1]
    final_state = jnp.sum(drive * jnp.exp(total_log[None] - running), axis=0)
    return ((jnp.exp(total_log), final_state), running)


def finish(decay, drive, incoming, reverse):
    if reverse:
        seeded = jnp.concatenate([drive[:-1], drive[-1:] + decay[-1:] * incoming[None]], axis=0)
    else:
        seeded = jnp.concatenate([drive[:1] + decay[:1] * incoming[None], drive[1:]], axis=0)
    return lax.associative_scan(compose, (decay, seeded), axis=0, reverse=reverse)[1]


def shards(
    tokens, norm_gain, x_weight, gate_weight, conv_taps, rate_map, input_map, decay_rate, out_weight
):
    flt = tokens.astype(jnp.float32)
    scale = lax.rsqrt(jnp.mean(flt * flt, axis=-1, keepdims=True) + epsilon)
    normed = (flt * scale * norm_gain).astype(jnp.bfloat16)
    channels = x_weight.shape[1]
    joined = jnp.concatenate([x_weight, gate_weight], axis=1)
    local_steps, seqs_here, width_in = normed.shape

    def add_rows(total, piece, start):
        columns = lax.dynamic_slice_in_dim(normed, start, piece.shape[0], 2)
        return total + jnp.einsum("tsd,dc->tsc", columns, piece, preferred_element_type=jnp.float32)

    empty = jnp.zeros((local_steps, seqs_here, 2 * channels), jnp.float32)
    projected = taken_in(joined, ("sp", "tp"), 0, add_rows, empty)
    branch = projected[..., :channels].astype(jnp.bfloat16)
    gate_in = projected[..., channels:].astype(jnp.bfloat16)
    full_rate, full_input = (
        lax.all_gather(rate_map, ("sp", "tp"), axis=1, tiled=True),
        lax.all_gather(input_map, ("sp", "tp"), axis=1, tiled=True),
    )
    block_width = full_rate.shape[2]
    nblk = channels // block_width
    full_rate = full_rate.reshape(2, nblk, block_width, block_width)
    full_input = full_input.reshape(2, nblk, block_width, block_width)
    extended = extended_2(branch, (("sp", 0),), 2, False)
    conv = extended[0:local_steps].astype(jnp.float32) * conv_taps[0]
    for offset in range(1, 4):
        conv = (
            conv + extended[offset : offset + local_steps].astype(jnp.float32) * conv_taps[offset]
        )
    conv_bf = lax.optimization_barrier(conv.astype(jnp.bfloat16))
    conv_f = conv_bf.astype(jnp.float32)
    seq_total = local_steps * lax.axis_size("sp")
    fwd_decay, fwd_drive, fwd_log = drive_terms(
        conv_bf, conv_f, full_rate[0], full_input[0], decay_rate[0], seq_total
    )
    bwd_decay, bwd_drive, bwd_log = drive_terms(
        conv_bf, conv_f, full_rate[1], full_input[1], decay_rate[1], seq_total
    )
    fwd_summary, fwd_kept = summarize(fwd_drive, fwd_log, False)
    bwd_summary, bwd_kept = summarize(bwd_drive, bwd_log, True)
    identity = (jnp.ones_like(fwd_summary[0]), jnp.zeros_like(fwd_summary[1]))
    fwd_incoming = carried_in(fwd_summary, "sp", compose, identity, False)[1]
    bwd_incoming = carried_in(bwd_summary, "sp", compose, identity, True)[1]
    forward = finish(fwd_decay, fwd_drive, fwd_incoming, False)
    backward = finish(bwd_decay, bwd_drive, bwd_incoming, True)
    recurrent = lax.optimization_barrier((forward + backward).astype(jnp.bfloat16))
    gated = (recurrent.astype(jnp.float32) * jax.nn.gelu(gate_in.astype(jnp.float32))).astype(
        jnp.bfloat16
    )

    def project(piece, start):
        return jnp.einsum("tsc,cd->tsd", gated, piece, preferred_element_type=jnp.float32).astype(
            jnp.bfloat16
        )

    return on_whole(out_weight, ("sp", "tp"), 1, project)


def solution(mesh):
    placed = (
        P("sp", "tp", None),
        P(),
        P(("sp", "tp"), None),
        P(("sp", "tp"), None),
        P(),
        P(None, ("sp", "tp"), None),
        P(None, ("sp", "tp"), None),
        P(),
        P(None, ("sp", "tp")),
    )
    return jax.shard_map(
        shards, mesh=mesh, in_specs=placed, out_specs=P("sp", "tp", None), check_vma=False
    )
```

profile of v0, /device:TPU:0, one launch (start us, length us, event | category | flops | bytes accessed | tf_op | source)
XLA Modules:
  0.0 490.6 jit_solution(9915394843487729214)
XLA Ops:
  11.7 45.6 %all_gather.33 = bf16[2,1024,128]{2,1,0:T(8,128)(2,1)S(1)} all-gather(bf16[2,32,128]{2,1,0:T(8,128)(2,1)} %param.18), channel_id=1, replica_groups=mesh['sp'=8,'tp'=4] {'sp','tp'}, dimensions={1}, use_global_device_ids=true | all-gather | bytes 540672 | tf_op jit(solution)/shard_map/all_gather | solution.py:106
  58.1 39.2 %all_gather.34 = bf16[2,1024,128]{2,1,0:T(8,128)(2,1)S(1)} all-gather(bf16[2,32,128]{2,1,0:T(8,128)(2,1)S(1)} %copy-done.41), channel_id=1, replica_groups=mesh['sp'=8,'tp'=4] {'sp','tp'}, dimensions={1}, use_global_device_ids=true | all-gather | bytes 540672 | tf_op jit(solution)/shard_map/all_gather | solution.py:107
  105.6 4.1 collective-permute-done.1
  125.9 5.1 %fusion.28 = (f32[12,1024]{1,0:T(8,128)S(1)}, f32[32,12,1024]{2,0,1:T(8,128)}, f32[12,1024]{1,0:T(8,128)S(1)}, f32[32,12,1024]{2,0,1:T(8,128)}) fusion(f32[32,12,1024]{2,1,0:T(8,128)S(1)} %fusion.11, f32[12,1024]{1,0:T(8,128)S(1)} %get-tuple-element.260, bf16[32,12,1024]{2,0,1:T(8,128)(2,1)S(1)} %copy-done.5, ...), kind=kLoop, calls=%fused_computation.46 | loop fusion | flops 6660096 | bytes 13574144 | tf_op jit(solution)/shard_map/reduce_sum | solution.py:75
  131.0 31.5 %all-gather.2 = f32[8,12,1024]{2,1,0:T(8,128)S(1)} all-gather(f32[1,12,1024]{2,1,0:T(8,128)S(1)} %bitcast.181), channel_id=2, replica_groups=mesh['sp'=8,'tp'=4] {'sp'}, dimensions={0}, use_global_device_ids=true | all-gather | bytes 442368 | tf_op jit(solution)/shard_map/all_gather | solution.py:33
  162.5 31.6 %all_gather.35 = f32[8,12,1024]{2,1,0:T(8,128)S(1)} all-gather(f32[1,12,1024]{2,1,0:T(8,128)S(1)} %get-tuple-element.259), channel_id=1, replica_groups=mesh['sp'=8,'tp'=4] {'sp'}, dimensions={0}, use_global_device_ids=true | all-gather | bytes 442368 | tf_op jit(solution)/shard_map/all_gather | solution.py:33
  194.4 31.3 %all-gather.3 = f32[8,12,1024]{2,1,0:T(8,128)S(1)} all-gather(f32[1,12,1024]{2,1,0:T(8,128)S(1)} %bitcast.180), channel_id=3, replica_groups=mesh['sp'=8,'tp'=4] {'sp'}, dimensions={0}, use_global_device_ids=true | all-gather | bytes 442368 | tf_op jit(solution)/shard_map/all_gather | solution.py:33
  225.7 31.4 %all_gather.38 = f32[8,12,1024]{2,1,0:T(8,128)S(1)} all-gather(f32[1,12,1024]{2,1,0:T(8,128)S(1)} %get-tuple-element.261), channel_id=1, replica_groups=mesh['sp'=8,'tp'=4] {'sp'}, dimensions={0}, use_global_device_ids=true | all-gather | bytes 442368 | tf_op jit(solution)/shard_map/all_gather | solution.py:33
  265.4 4.3 slice.341
  308.3 4.3 slice.384
  312.7 4.3 slice.386
  321.3 5.1 %slice.385 = f32[16,12,1024]{2,0,1:T(8,128)} reverse(f32[16,12,1024]{2,0,1:T(8,128)} %slice.384), dimensions={0} | reverse | bytes 1572864 | tf_op jit(solution)/shard_map/slice | solution.py:84
  326.3 5.0 %slice.387 = f32[16,12,1024]{2,0,1:T(8,128)} reverse(f32[16,12,1024]{2,0,1:T(8,128)} %slice.386), dimensions={0} | reverse | bytes 1572864 | tf_op jit(solution)/shard_map/slice | solution.py:84
  331.4 5.1 %slice.382 = f32[16,12,1024]{2,0,1:T(8,128)} reverse(f32[16,12,1024]{2,0,1:T(8,128)} %slice.381), dimensions={0} | reverse | bytes 1572864 | tf_op jit(solution)/shard_map/slice | solution.py:84
  336.5 5.1 %slice.390 = f32[16,12,1024]{2,0,1:T(8,128)} reverse(f32[16,12,1024]{2,0,1:T(8,128)} %slice.389), dimensions={0} | reverse | bytes 1572864 | tf_op jit(solution)/shard_map/slice | solution.py:84
  388.0 4.4 slice.338
  420.7 5.3 %pad.71 = f32[32,12,1024]{2,0,1:T(8,128)S(1)} pad(f32[16,12,1024]{2,0,1:T(8,128)} %add.255, f32[]{:T(128)} %constant.72.clone.1), padding=1_0_1x0_0_0x0_0_0 | pad | bytes 2359300 | tf_op jit(solution)/shard_map/pad | solution.py:84
  427.9 5.3 %pad.70 = f32[32,12,1024]{2,0,1:T(8,128)} pad(f32[16,12,1024]{2,0,1:T(8,128)S(1)} %pad_maximum_fusion.4, f32[]{:T(128)} %constant.72.clone.1), padding=0_1_1x0_0_0x0_0_0 | pad | bytes 2359300 | tf_op jit(solution)/shard_map/pad | solution.py:84
  439.1 8.2 %pad.81 = f32[32,12,1024]{2,0,1:T(8,128)} pad(f32[16,12,1024]{2,0,1:T(8,128)} %add.272, f32[]{:T(128)} %constant.72.clone.1), padding=1_0_1x0_0_0x0_0_0 | pad | bytes 2359300 | tf_op jit(solution)/shard_map/pad | solution.py:84
  447.3 5.1 %slice.419 = f32[15,12,1024]{2,0,1:T(8,128)} reverse(f32[15,12,1024]{2,0,1:T(8,128)} %slice.418), dimensions={0} | reverse | bytes 1474560 | tf_op jit(solution)/shard_map/slice | solution.py:84
  452.4 5.1 %slice.380 = f32[15,12,1024]{2,0,1:T(8,128)} reverse(f32[15,12,1024]{2,0,1:T(8,128)} %slice.379), dimensions={0} | reverse | bytes 1474560 | tf_op jit(solution)/shard_map/slice | solution.py:84
  460.2 8.1 %pad.80 = f32[32,12,1024]{2,0,1:T(8,128)} pad(f32[16,12,1024]{2,0,1:T(8,128)} %pad_maximum_fusion.5, f32[]{:T(128)} %constant.72.clone.1), padding=0_1_1x0_0_0x0_0_0 | pad | bytes 2359300 | tf_op jit(solution)/shard_map/pad | solution.py:84
  471.3 5.6 %rev.13 = f32[32,12,1024]{2,0,1:T(8,128)} reverse(f32[32,12,1024]{2,0,1:T(8,128)} %add.274), dimensions={0} | reverse | bytes 3145728 | tf_op jit(solution)/shard_map/rev | solution.py:84
  479.5 4.2 fusion.29
  (234 shorter events, 172.1 us)
Async XLA Ops:
  6.5 51.6 %copy-start.41 = (bf16[2,32,128]{2,1,0:T(8,128)(2,1)S(1)}, bf16[2,32,128]{2,1,0:T(8,128)(2,1)}, u32[]{:S(2)}) copy-start(bf16[2,32,128]{2,1,0:T(8,128)(2,1)} %param.19) | copy-start | bytes 49156
  6.5 91.7 %all-gather.7.cloned.1.call-start = ((), (), s32[]{:S(2)}) async-start(), calls=%async_computation | async-start | bytes 4325376 | tf_op jit(solution)/shard_map/all_gather | solution.py:10
  8.1 471.4 %all-gather.9.cloned.1.call-start = ((), (), s32[]{:S(2)}) async-start(), calls=%async_computation.1 | async-start | bytes 2162688 | tf_op jit(solution)/shard_map/all_gather | solution.py:49
  11.7 86.5 %copy-start.14 = (bf16[32,12,1024]{2,0,1:T(8,128)(2,1)S(1)}, bf16[32,12,1024]{2,0,1:T(8,128)(2,1)}, u32[]{:S(2)}) copy-start(bf16[32,12,1024]{2,0,1:T(8,128)(2,1)} %param.13) | copy-start | bytes 2359300
  11.7 86.5 %copy-start.43 = (f32[1024]{0:T(1024)S(1)}, f32[1024]{0:T(1024)}, u32[]{:S(2)}) copy-start(f32[1024]{0:T(1024)} %param.14) | copy-start | bytes 12292
  98.2 7.0 %copy-start.42 = (f32[2,1024]{1,0:T(2,128)S(1)}, f32[2,1024]{1,0:T(2,128)}, u32[]{:S(2)}) copy-start(f32[2,1024]{1,0:T(2,128)} %param.20) | copy-start | bytes 24580
  102.3 9.8 %copy-start.20 = (bf16[32,12,2048]{2,0,1:T(8,128)(2,1)}, bf16[32,12,2048]{2,0,1:T(8,128)(2,1)S(1)}, u32[]{:S(2)}) copy-start(bf16[32,12,2048]{2,0,1:T(8,128)(2,1)S(1)} %fusion.4) | copy-start | bytes 4718596
  102.4 3.2 collective-permute-start
  103.7 6.0 %collective-permute-start.1 = (bf16[2,12,1024]{2,0,1:T(2,128)(2,1)S(1)}, bf16[2,12,1024]{2,0,1:T(2,128)(2,1)S(1)}, u32[]{:S(2)}, u32[]{:S(2)}) collective-permute-start(bf16[2,12,1024]{2,0,1:T(2,128)(2,1)S(1)} %get-tuple-element.263), channel_id=1, source_target_pairs={{4,0},{8,4},{12,8},{16,12},{20,16},{24,20},{28,24},{5,1},{9,5},{13... | collective-permute-start | bytes 147464 | tf_op jit(solution)/shard_map/ppermute | solution.py:24
  105.2 6.9 %copy-start.32 = (bf16[1,1024,128]{2,1,0:T(8,128)(2,1)S(1)}, bf16[1,1024,128]{2,1,0:T(8,128)(2,1)}, u32[]{:S(2)}) copy-start(bf16[1,1024,128]{2,1,0:T(8,128)(2,1)} %get-tuple-element.273) | copy-start | bytes 786436
  114.6 4.4 copy-start
  388.0 4.4 copy-start.11
  388.0 15.6 %copy-start.6 = (f32[8,12,1024]{2,0,1:T(8,128)S(1)}, f32[8,12,1024]{2,0,1:T(8,128)}, u32[]{:S(2)}) copy-start(f32[8,12,1024]{2,0,1:T(8,128)} %get-tuple-element.278) | copy-start | bytes 1179652
  393.8 18.9 %copy-start.1 = (f32[32,12,1024]{2,0,1:T(8,128)S(1)}, f32[32,12,1024]{2,0,1:T(8,128)}, u32[]{:S(2)}) copy-start(f32[32,12,1024]{2,0,1:T(8,128)} %pad_maximum_fusion.1) | copy-start | bytes 4718596
  412.7 4.3 copy-start.38
  412.7 4.7 copy-start.25
  412.7 4.7 copy-start.27
  427.9 5.3 %copy-start.19 = (f32[2,12,1024]{2,0,1:T(2,128)S(1)}, f32[2,12,1024]{2,0,1:T(2,128)}, u32[]{:S(2)}) copy-start(f32[2,12,1024]{2,0,1:T(2,128)} %slice.404) | copy-start | bytes 294916
  427.9 5.3 %copy-start.28 = (f32[2,12,1024]{2,0,1:T(2,128)S(1)}, f32[2,12,1024]{2,0,1:T(2,128)}, u32[]{:S(2)}) copy-start(f32[2,12,1024]{2,0,1:T(2,128)} %slice.406) | copy-start | bytes 294916
  427.9 5.3 %copy-start.29 = (f32[2,12,1024]{2,0,1:T(2,128)S(1)}, f32[2,12,1024]{2,0,1:T(2,128)}, u32[]{:S(2)}) copy-start(f32[2,12,1024]{2,0,1:T(2,128)} %slice.405) | copy-start | bytes 294916
  427.9 5.4 %copy-start.33 = (f32[2,12,1024]{2,0,1:T(2,128)S(1)}, f32[2,12,1024]{2,0,1:T(2,128)}, u32[]{:S(2)}) copy-start(f32[2,12,1024]{2,0,1:T(2,128)} %slice.408) | copy-start | bytes 294916
  427.9 5.5 %copy-start.12 = (f32[8,6,1024]{2,0,1:T(8,128)S(1)}, f32[8,6,1024]{2,0,1:T(8,128)}, u32[]{:S(2)}) copy-start(f32[8,6,1024]{2,0,1:T(8,128)} %get-tuple-element.310) | copy-start | bytes 589828
  460.2 8.1 %copy-start.3 = (f32[32,12,1024]{2,0,1:T(8,128)S(1)}, f32[32,12,1024]{2,0,1:T(8,128)}, u32[]{:S(2)}) copy-start(f32[32,12,1024]{2,0,1:T(8,128)} %pad.81) | copy-start | bytes 4718596
  471.3 5.6 %copy-start.2 = (f32[32,12,1024]{2,0,1:T(8,128)S(1)}, f32[32,12,1024]{2,0,1:T(8,128)}, u32[]{:S(2)}) copy-start(f32[32,12,1024]{2,0,1:T(8,128)} %pad.70) | copy-start | bytes 4718596
  (24 other events, 45.7 us)
Sparse Core Ops, SparseCore 0:
  10.2 66.8 all-gather.6
  79.9 54.8 all-gather.8
where the time goes:
time: 496 us; the launch traced here: 491 us
  blocking collectives  211 us (43%)
  local copies, waits for them, and re-layouts  189 us (38%)
  other arithmetic  57.5 us (12%)
  between operations  14.2 us (3%)
  matrix products  10.6 us (2%)
  waiting for transfers between devices  5.08 us (1%)
    slice x54, local copies, waits for them, and re-layouts, finish(): lax.associative_scan(compose, (decay, seeded), axis=0, reverse=reverse)[1]  146 us
    all_gather x4, blocking collectives, carried_in(): pieces = jax.tree.map(lambda part: lax.all_gather(part, axis), value)  126 us
    all_gather x1, blocking collectives, shards(): lax.all_gather(rate_map, ('sp', 'tp'), axis=1, tiled=True)  45.6 us
    all_gather x1, blocking collectives, shards(): lax.all_gather(input_map, ('sp', 'tp'), axis=1, tiled=True)  39.2 us
    pad x16, local copies, waits for them, and re-layouts, finish(): lax.associative_scan(compose, (decay, seeded), axis=0, reverse=reverse)[1]  29.4 us
    mul x6, other arithmetic, compose(): return (earlier[0] * later[0], later[0] * earlier[1] + later[1])  15.4 us
  transfers between devices with their start and end apart: 4, of which 2 were waited for; matrix products, arithmetic and copies ran while one was open for 51% of the time, Pallas kernels for 0%

commit v1 on v0

v1 whole, which is shorter than its diff:
```python
import functools

import jax
import jax.numpy as jnp
from jax import lax
from jax.experimental import pallas as pl
from jax.experimental.pallas import tpu as pltpu
from jax.sharding import PartitionSpec as P

epsilon = 1e-06
MESH = pl.DeviceIdType.MESH
f32, bf16 = jnp.float32, jnp.bfloat16
ROWS = 64
COLS = 256


class Gather:
    def __init__(self, grid, place, order, own, buf, send, recv, local):
        self.grid, self.place, self.order = grid, place, order
        self.own, self.buf, self.send, self.recv, self.local = own, buf, send, recv, local
        self.copies, self.base = {}, 0
        self.bases = []
        count = 0
        for axis in order:
            self.bases.append(count)
            count += grid[axis] - 1

    def slab(self, done):
        return self.buf.at[
            tuple(
                pl.ds(0, self.grid[a]) if a in done else pl.ds(self.place[a], 1) for a in range(4)
            )
        ]

    def start(self, phase):
        axis = self.order[phase]
        made = []
        if phase == 0:
            self.kept = pltpu.make_async_copy(
                self.own, self.buf.at[tuple(self.place)], self.local
            )
            self.kept.start()
        for o in range(1, self.grid[axis]):
            there = list(self.place)
            there[axis] = lax.rem(self.place[axis] + o, self.grid[axis])
            if phase == 0:
                src, dst = self.own, self.buf.at[tuple(self.place)]
            else:
                src = dst = self.slab(self.order[:phase])
            at = self.bases[phase] + o - 1
            made.append(
                pltpu.make_async_remote_copy(
                    src_ref=src,
                    dst_ref=dst,
                    send_sem=self.send.at[at],
                    recv_sem=self.recv.at[at],
                    device_id=device(self.grid, there),
                    device_id_type=MESH,
                )
            )
            made[-1].start()
        self.copies[phase] = made

    def wait(self, phase):
        if phase == 0:
            self.kept.wait()
        for copy in self.copies[phase]:
            copy.wait_recv()

    def drain(self):
        for made in self.copies.values():
            for copy in made:
                copy.wait_send()


def device(grid, place):
    return (place[0] * grid[1] + place[1], place[2] * grid[3] + place[3])


def kernel(
    grid, gathered, seq_total, names, tok, gain, taps, speed, x_w, maps, g_w, o_w, out, *scratch
):
    r = dict(zip(names, scratch))
    n_sp = grid[0] * grid[1]
    sp, tp = lax.axis_index("sp"), lax.axis_index("tp")
    z, y = sp // grid[1], lax.rem(sp, grid[1])
    x, c = tp // grid[3], lax.rem(tp, grid[3])
    place = [z, y, x, c]
    steps, seqs, channels = r["rec"].shape
    width = tok.shape[1]
    total_rows = tok.shape[0]
    nblk, bw = r["mb"].shape[0] if gathered else maps.shape[0], 128

    barrier = pltpu.get_barrier_semaphore()
    greeted = 0
    for axis in range(4):
        if axis >= 2 and not gathered:
            continue
        for o in range(1, grid[axis]):
            there = list(place)
            there[axis] = lax.rem(place[axis] + o, grid[axis])
            pl.semaphore_signal(
                barrier, inc=1, device_id=device(grid, there), device_id_type=MESH
            )
            greeted += 1
    before, after = lax.rem(sp + n_sp - 1, n_sp), lax.rem(sp + 1, n_sp)
    for there in (before, after):
        pl.semaphore_signal(barrier, inc=1, device_id=(there, tp), device_id_type=MESH)
        greeted += 1
    pl.semaphore_wait(barrier, greeted)

    if gathered:
        outward, inward = (2, 1, 0, 3), (0, 1, 2, 3)
        gx, gm, gg, go = (
            Gather(grid, place, order, own, r[name], r["send"].at[i], r["recv"].at[i], r["local"].at[i])
            for i, (name, order, own) in enumerate(
                (("wx", outward, x_w), ("wm", inward, maps), ("wg", inward, g_w), ("wo", outward, o_w))
            )
        )
        gx.start(0)
        gm.start(0)
        gg.start(0)

    def advance(g, phase):
        if gathered:
            g.wait(phase)
            if phase < 3:
                g.start(phase + 1)

    if not gathered:
        gx = gm = gg = go = None

    def norm_rows(i, _):
        rows = pl.ds(pl.multiple_of(i * ROWS, ROWS), ROWS)
        flt = tok[rows, :].astype(f32)
        scale = lax.rsqrt(jnp.mean(flt * flt, axis=-1, keepdims=True) + epsilon)
        r["normed"][rows, :] = (flt * scale * gain[...]).astype(bf16)
        return 0

    half = total_rows // ROWS // 2
    lax.fori_loop(0, half, norm_rows, 0)
    advance(gx, 0)
    lax.fori_loop(half, total_rows // ROWS, norm_rows, 0)
    advance(gx, 1)
    advance(gm, 0)
    advance(gg, 0)
    advance(gm, 1)
    advance(gx, 2)
    if gathered:
        go.start(0)
    advance(gm, 2)
    advance(gx, 3)

    def columns_of(name, ref, at):
        if gathered:
            return r[name][:, :, :, :, :, pl.ds(at, COLS)].reshape(width, COLS)
        return ref[:, pl.ds(at, COLS)]

    def project_branch(i, _):
        at = pl.multiple_of(i * COLS, COLS)
        piece = jnp.dot(
            r["normed"][...], columns_of("wx", x_w, at), preferred_element_type=f32
        ).astype(bf16)
        r["br"][pl.ds(2, steps), :, pl.ds(at, COLS)] = piece.reshape(steps, seqs, COLS)
        return 0

    lax.fori_loop(0, channels // COLS, project_branch, 0)
    head = pltpu.make_async_remote_copy(
        src_ref=r["br"].at[pl.ds(2, 1)],
        dst_ref=r["hi"],
        send_sem=r["hsend"].at[0],
        recv_sem=r["hrecv"].at[0],
        device_id=(before, tp),
        device_id_type=MESH,
    )
    tail = pltpu.make_async_remote_copy(
        src_ref=r["br"].at[pl.ds(steps, 2)],
        dst_ref=r["lo"],
        send_sem=r["hsend"].at[1],
        recv_sem=r["hrecv"].at[1],
        device_id=(after, tp),
        device_id_type=MESH,
    )
    head.start()
    tail.start()
    advance(gm, 3)
    if gathered:
        slab_rows = maps.shape[1]
        for d in range(nblk * bw // slab_rows):
            s, t = divmod(d, grid[2] * grid[3])
            at = (s // grid[1], s % grid[1], t // grid[3], t % grid[3])
            block, low = divmod(d * slab_rows, bw)
            for k in range(4):
                r["mb"][block, low : low + slab_rows, k * bw : (k + 1) * bw] = r["wm"][at + (k,)]
    head.wait_recv()
    tail.wait_recv()
    r["br"][0:2] = jnp.where(sp > 0, r["lo"][...], jnp.zeros_like(r["lo"]))
    r["br"][steps + 2 : steps + 3] = jnp.where(
        sp < n_sp - 1, r["hi"][...], jnp.zeros_like(r["hi"])
    )
    advance(gg, 1)
    advance(go, 0)

    group = 4

    def terms(i, k, lanes):
        t = pl.ds(pl.multiple_of(i * group, group), group)
        rate = 0.5 * jnp.tanh(0.5 * r["gates"][t, :, k * bw : (k + 1) * bw]) + 0.5
        inp = 0.5 * jnp.tanh(0.5 * r["gates"][t, :, (k + 2) * bw : (k + 3) * bw]) + 0.5
        factor = (speed[k : k + 1, lanes] * (-2.0 / seq_total)).reshape(1, 1, bw)
        log_decay = rate * factor
        decay = jnp.exp(log_decay)
        u = 2.0 * log_decay
        gone = -u * (1.0 + u * (1 / 2 + u * (1 / 6 + u * (1 / 24 + u * (1 / 120)))))
        root = gone * lax.rsqrt(jnp.maximum(gone, 1e-37))
        return decay, root * inp * r["cf"][t].astype(f32)

    def block_step(b, _):
        lanes = pl.ds(pl.multiple_of(b * bw, bw), bw)

        def conv_rows(i, _):
            t0 = i * group
            conv = r["br"][pl.ds(t0, group), :, lanes].astype(f32) * taps[0:1, lanes].reshape(1, 1, bw)
            for j in range(1, 4):
                conv = conv + r["br"][pl.ds(t0 + j, group), :, lanes].astype(f32) * taps[
                    j : j + 1, lanes
                ].reshape(1, 1, bw)
            r["cf"][pl.ds(t0, group)] = conv.astype(bf16)
            return 0

        lax.fori_loop(0, steps // group, conv_rows, 0)
        mat = r["mb"][b] if gathered else maps[b]
        r["gates"][...] = jnp.dot(
            r["cf"][...].reshape(steps * seqs, bw), mat, preferred_element_type=f32
        ).reshape(steps, seqs, 4 * bw)

        def forward(i, carry):
            prod, state = carry
            decay, drive = terms(i, 0, lanes)
            for j in range(group):
                prod = prod * decay[j]
                state = state * decay[j] + drive[j]
                r["pf"][i * group + j, :, lanes] = prod
                r["rec"][i * group + j, :, lanes] = state
            return prod, state

        one, zero = jnp.ones((seqs, bw), f32), jnp.zeros((seqs, bw), f32)
        prod, state = lax.fori_loop(0, steps // group, forward, (one, zero))
        r["sum"][0, 0, :, lanes] = prod
        r["sum"][0, 1, :, lanes] = state

        def backward(i, carry):
            prod, state = carry
            i = steps // group - 1 - i
            decay, drive = terms(i, 1, lanes)
            for j in reversed(range(group)):
                prod = prod * decay[j]
                state = state * decay[j] + drive[j]
                r["pb"][i * group + j, :, lanes] = prod
                r["rec"][i * group + j, :, lanes] += state
            return prod, state

        prod, state = lax.fori_loop(0, steps // group, backward, (one, zero))
        r["sum"][1, 0, :, lanes] = prod
        r["sum"][1, 1, :, lanes] = state
        return 0

    lax.fori_loop(0, nblk // 2, block_step, 0)
    advance(gg, 2)
    advance(go, 1)
    lax.fori_loop(nblk // 2, nblk, block_step, 0)

    mates = []
    for o in range(1, grid[1]):
        there = list(place)
        there[1] = lax.rem(y + o, grid[1])
        mates.append(
            pltpu.make_async_remote_copy(
                src_ref=r["sum"],
                dst_ref=r["mate"].at[o - 1],
                send_sem=r["ysend"].at[o - 1],
                recv_sem=r["yrecv"].at[o - 1],
                device_id=device(grid, there),
                device_id_type=MESH,
            )
        )
        mates[-1].start()
    advance(gg, 3)

    def project_gate(i, _):
        at = pl.multiple_of(i * COLS, COLS)
        piece = jnp.dot(
            r["normed"][...], columns_of("wg", g_w, at), preferred_element_type=f32
        ).astype(bf16)
        r["gate"][:, pl.ds(at, COLS)] = piece
        return 0

    lax.fori_loop(0, channels // COLS // 2, project_gate, 0)
    for copy in mates:
        copy.wait_recv()
    first = y == 0
    mine = [[r["sum"][k, q] for q in range(2)] for k in range(2)]
    theirs = [[r["mate"][0, k, q] for q in range(2)] for k in range(2)]
    for k in range(2):
        mine_first = first if k == 0 else jnp.logical_not(first)
        r["pair"][k, 0] = mine[k][0] * theirs[k][0]
        r["pair"][k, 1] = jnp.where(
            mine_first,
            theirs[k][0] * mine[k][1] + theirs[k][1],
            mine[k][0] * theirs[k][1] + mine[k][1],
        )
    across = []
    for o in range(1, grid[0]):
        there = list(place)
        there[0] = lax.rem(z + o, grid[0])
        way = (z + o) // grid[0]
        across.append(
            pltpu.make_async_remote_copy(
                src_ref=r["pair"].at[way],
                dst_ref=r["far"].at[o - 1],
                send_sem=r["zsend"].at[o - 1],
                recv_sem=r["zrecv"].at[o - 1],
                device_id=device(grid, there),
                device_id_type=MESH,
            )
        )
        across[-1].start()
    lax.fori_loop(channels // COLS // 2, channels // COLS, project_gate, 0)

    advance(go, 2)
    for copy in across:
        copy.wait_recv()
    hf = jnp.zeros((seqs, channels), f32)
    for o in range(grid[0] - 1, 0, -1):
        longer = r["far"][o - 1, 0] * hf + r["far"][o - 1, 1]
        hf = jnp.where(o <= z, longer, hf)
    hf = jnp.where(first, hf, r["mate"][0, 0, 0] * hf + r["mate"][0, 0, 1])
    r["hf"][...] = hf
    hb = jnp.zeros((seqs, channels), f32)
    for o in range(1, grid[0]):
        longer = r["far"][o - 1, 0] * hb + r["far"][o - 1, 1]
        hb = jnp.where(o > z, longer, hb)
    hb = jnp.where(first, r["mate"][0, 1, 0] * hb + r["mate"][0, 1, 1], hb)
    r["hb"][...] = hb

    def finish(i, _):
        rows = pl.ds(pl.multiple_of(i * seqs, seqs), seqs)
        for low in range(0, channels, COLS):
            lanes = pl.ds(low, COLS)
            recurrent = (
                r["rec"][i, :, lanes]
                + r["pf"][i, :, lanes] * r["hf"][:, lanes]
                + r["pb"][i, :, lanes] * r["hb"][:, lanes]
            ).astype(bf16).astype(f32)
            g = r["gate"][rows, lanes].astype(f32)
            inner = 0.7978845608028654 * (g + 0.044715 * (g * g * g))
            r["gated"][rows, lanes] = (
                recurrent * (g * (0.5 * (1.0 + jnp.tanh(inner))))
            ).astype(bf16)
        return 0

    lax.fori_loop(0, steps, finish, 0)
    advance(go, 3)
    o_tiles = grid[0] if gathered else width // COLS

    def project_out(i, _):
        wide = width // o_tiles
        at = pl.multiple_of(i * wide, 128)
        if gathered:
            mat = r["wo"][pl.ds(i, 1)].reshape(wide, channels)
            dims = (((1,), (1,)), ((), ()))
        else:
            mat = o_w[:, pl.ds(at, wide)]
            dims = (((1,), (0,)), ((), ()))
        piece = lax.dot_general(r["gated"][...], mat, dims, preferred_element_type=f32)
        out[:, pl.ds(at, wide)] = piece.astype(bf16)
        return 0

    lax.fori_loop(0, o_tiles, project_out, 0)
    head.wait_send()
    tail.wait_send()
    for copy in mates + across:
        copy.wait_send()
    if gathered:
        for g in (gx, gm, gg, go):
            g.drain()


def shards(
    sizes, tokens, norm_gain, x_weight, gate_weight, conv_taps, rate_map, input_map, decay_rate, out_weight
):
    n_sp, n_tp = sizes
    grid = (n_sp // 2, 2, n_tp // 2, 2)
    steps, seqs_here, width = tokens.shape
    channels = x_weight.shape[1]
    slab = x_weight.shape[0]
    bw = rate_map.shape[2]
    nblk = channels // bw
    seqs = -(-seqs_here // 16) * 16
    gathered = slab % 16 == 0
    tok = jnp.pad(tokens, ((0, 0), (0, seqs - seqs_here), (0, 0))).reshape(steps * seqs, width)
    maps = jnp.concatenate([rate_map, input_map], axis=0)
    if gathered:
        x_w, g_w, o_w = x_weight, gate_weight, out_weight.T
    else:
        both = ("sp", "tp")
        x_w = lax.all_gather(x_weight, both, axis=0, tiled=True)
        g_w = lax.all_gather(gate_weight, both, axis=0, tiled=True)
        o_w = lax.all_gather(out_weight, both, axis=1, tiled=True)
        maps = lax.all_gather(maps, both, axis=1, tiled=True)
        maps = maps.reshape(4, nblk, bw, bw).transpose(1, 2, 0, 3).reshape(nblk, bw, 4 * bw)

    spec = {
        "normed": pltpu.VMEM((steps * seqs, width), bf16),
        "br": pltpu.VMEM((steps + 3, seqs, channels), bf16),
        "lo": pltpu.VMEM((2, seqs, channels), bf16),
        "hi": pltpu.VMEM((1, seqs, channels), bf16),
        "cf": pltpu.VMEM((steps, seqs, bw), bf16),
        "gates": pltpu.VMEM((steps, seqs, 4 * bw), f32),
        "rec": pltpu.VMEM((steps, seqs, channels), f32),
        "pf": pltpu.VMEM((steps, seqs, channels), f32),
        "pb": pltpu.VMEM((steps, seqs, channels), f32),
        "gate": pltpu.VMEM((steps * seqs, channels), bf16),
        "gated": pltpu.VMEM((steps * seqs, channels), bf16),
        "sum": pltpu.VMEM((2, 2, seqs, channels), f32),
        "pair": pltpu.VMEM((2, 2, seqs, channels), f32),
        "mate": pltpu.VMEM((grid[1] - 1, 2, 2, seqs, channels), f32),
        "far": pltpu.VMEM((grid[0] - 1, 2, seqs, channels), f32),
        "hf": pltpu.VMEM((seqs, channels), f32),
        "hb": pltpu.VMEM((seqs, channels), f32),
        "hsend": pltpu.SemaphoreType.DMA((2,)),
        "hrecv": pltpu.SemaphoreType.DMA((2,)),
        "ysend": pltpu.SemaphoreType.DMA((grid[1] - 1,)),
        "yrecv": pltpu.SemaphoreType.DMA((grid[1] - 1,)),
        "zsend": pltpu.SemaphoreType.DMA((grid[0] - 1,)),
        "zrecv": pltpu.SemaphoreType.DMA((grid[0] - 1,)),
    }
    if gathered:
        hops = sum(grid) - 4
        spec |= {
            "wx": pltpu.VMEM(grid + (slab, channels), bf16),
            "wg": pltpu.VMEM(grid + (slab, channels), bf16),
            "wo": pltpu.VMEM(grid + (slab, channels), bf16),
            "wm": pltpu.VMEM(grid + (4, slab, bw), bf16),
            "mb": pltpu.VMEM((nblk, bw, 4 * bw), bf16),
            "send": pltpu.SemaphoreType.DMA((4, hops)),
            "recv": pltpu.SemaphoreType.DMA((4, hops)),
            "local": pltpu.SemaphoreType.DMA((4,)),
        }
    out = pl.pallas_call(
        functools.partial(kernel, grid, gathered, steps * n_sp, tuple(spec)),
        out_shape=jax.ShapeDtypeStruct((steps * seqs, width), bf16),
        in_specs=[pl.BlockSpec(memory_space=pltpu.VMEM)] * 8,
        out_specs=pl.BlockSpec(memory_space=pltpu.VMEM),
        scratch_shapes=list(spec.values()),
        compiler_params=pltpu.CompilerParams(
            collective_id=0, has_side_effects=True, vmem_limit_bytes=60 * 1024 * 1024
        ),
    )(tok, norm_gain.reshape(1, width), conv_taps, decay_rate, x_w, maps, g_w, o_w)
    return out.reshape(steps, seqs, width)[:, :seqs_here]


def solution(mesh):
    placed = (
        P("sp", "tp", None),
        P(),
        P(("sp", "tp"), None),
        P(("sp", "tp"), None),
        P(),
        P(None, ("sp", "tp"), None),
        P(None, ("sp", "tp"), None),
        P(),
        P(None, ("sp", "tp")),
    )
    return jax.shard_map(
        functools.partial(shards, (mesh.shape["sp"], mesh.shape["tp"])),
        mesh=mesh,
        in_specs=placed,
        out_specs=P("sp", "tp", None),
        check_vma=False,
    )
```

time: 496 us -> 105 us (0.21); the launches traced: 491 us -> 105 us
  blocking collectives: 211 us -> 0 us
  local copies, waits for them, and re-layouts: 189 us -> 5.27 us
  Pallas kernels: 0 us -> 98.2 us
  other arithmetic: 57.5 us -> 1.35 us
  between operations: 14.2 us -> 0.02 us
  matrix products: 10.6 us -> 0 us
  waiting for transfers between devices: 5.08 us -> 0 us
    all_gather x6 -> x0, blocking collectives: 211 us -> none  [the longest x4 126 us: carried_in(): pieces = jax.tree.map(lambda part: lax.all_gather(part, axis), value)]
    slice x60 -> x0, local copies, waits for them, and re-layouts: 151 us -> none  [the longest x54 146 us: finish(): lax.associative_scan(compose, (decay, seeded), axis=0, reverse=reverse)[1]]
    pallas_call x0 -> x1, Pallas kernels: none -> 98.2 us  [shards(): pl.pallas_call(functools.partial(kernel, grid, gathered, steps * n_sp, tu...]
    pad x16 -> x1, local copies, waits for them, and re-layouts: 29.4 us -> 1.16 us  [shards(): jnp.pad(tokens, ((0, 0), (0, seqs - seqs_here), (0, 0)))]
    mul x7 -> x0, other arithmetic: 15.4 us -> none  [the longest x6 15.4 us: compose(): return (earlier[0] * later[0], later[0] * earlier[1] + later[1])]
    add x20 -> x0, other arithmetic: 13.3 us -> none  [the longest x10 5.99 us: compose(): return (earlier[0] * later[0], later[0] * earlier[1] + later[1])]
    dot_general x6 -> x0, matrix products: 10.6 us -> none  [the longest x1 4.25 us: project(): jnp.einsum('tsc,cd->tsd', gated, piece, preferred_element_type=jnp.float32)]
    concatenate x11 -> x1, other arithmetic: 8.42 us -> 1.35 us  [shards(): maps = jnp.concatenate([rate_map, input_map], axis=0)]
  transfers between devices with their start and end apart: 4 -> 0, of which waited for: 2 -> 0; matrix products, arithmetic and copies ran while one was open for 51% -> 0% of each run, Pallas kernels for 0% -> 0%
where the time goes in v1:
time: 105 us
  Pallas kernels  98.2 us (94%)
  local copies, waits for them, and re-layouts  5.27 us (5%)
  other arithmetic  1.35 us (1%)
    pallas_call x1, Pallas kernels, shards(): pl.pallas_call(functools.partial(kernel, grid, gathered, steps * n_sp, tu...  98.2 us
    unnamed x2, local copies, waits for them, and re-layouts  4.12 us

profile of v1, /device:TPU:0, one launch (start us, length us, event | category | flops | bytes accessed | tf_op | source)
XLA Modules:
  0.0 104.9 jit_solution(618329501874848847)
XLA Ops:
  0.0 1.4 %pad_maximum_fusion.maps = bf16[4,32,128]{2,1,0:T(8,128)(2,1)} fusion(bf16[2,32,128]{2,1,0:T(8,128)(2,1)} %param.15, bf16[2,32,128]{2,1,0:T(8,128)(2,1)} %param.14), kind=kLoop, calls=%fused_computation | loop fusion | flops 16384 | bytes 65536 | tf_op jit(solution)/shard_map/concatenate | solution.py:402
  1.4 1.6 %copy.13 = bf16[32,12,1024]{2,1,0:T(8,128)(2,1)S(1)} copy(bf16[32,12,1024]{2,0,1:T(8,128)(2,1)} %param.9) | data formatting | bytes 1572864
  2.9 1.2 %pad.4.clone = bf16[32,16,1024]{2,1,0:T(8,128)(2,1)} pad(bf16[32,12,1024]{2,1,0:T(8,128)(2,1)S(1)} %copy.13, bf16[]{:T(256)} %constant.2.clone.1), padding=0_0x0_4x0_0 | pad | bytes 1835010 | tf_op jit(solution)/shard_map/jit(_pad)/pad | solution.py:401
  4.1 98.2 %shard_map.91 = bf16[512,1024]{1,0:T(8,128)(2,1)} custom-call(bf16[512,1024]{1,0:T(8,128)(2,1)} %bitcast.5, f32[1,1024]{1,0:T(1,128)} %bitcast.8, f32[4,1024]{1,0:T(4,128)} %taps.1, f32[2,1024]{1,0:T(2,128)} %speed.1, bf16[32,1024]{1,0:T(8,128)(2,1)} %x_w.1, bf16[4,32,128]{2,1,0:T(8,128)(2,1)} %pad_maximum_fusion.maps, bf16[32,1024]{1,0:T(8,128)(2,1)} %g_w.1, ...), custom_call_target="tpu_custom_call" | custom-call | tf_op jit(solution)/shard_map/pallas_call | solution.py:450
  102.3 2.5 %copy.12 = bf16[32,12,1024]{2,0,1:T(8,128)(2,1)} copy(bf16[32,12,1024]{2,1,0:T(8,128)(2,1)} %bitcast.6) | data formatting | bytes 1572864
